TPU v7x, 32 devices: a whole 2x2x4 slice. The times are simulated.
32 devices in a mesh: sp: 8 (over z, x), tp: 4 (over y, core).
Axes of the slice: x: 2, y: 2, z: 4, core: 2. Of those that a mesh axis runs over, the one named last changes fastest.
Arguments:
- tokens: bfloat16 [1024, 2048], P('sp', 'tp'), may hold values from -6 to 6
- conv_value_weight: bfloat16 [2048, 1024], P('sp', 'tp'), may hold values from -0.125 to 0.125
- conv_gate_weight: bfloat16 [2048, 1024], P('sp', 'tp'), may hold values from -0.125 to 0.125
- conv_kernel: bfloat16 [31, 1024], P(None, 'tp'), may hold values from -16 to 16
- conv_norm_gain: float32 [1024], P('tp'), may hold values from 0.1 to 1.9
- query_weight: bfloat16 [2048, 2048], P('sp', 'tp'), may hold values from -0.125 to 0.125
- key_weight: bfloat16 [2048, 2048], P('sp', 'tp'), may hold values from -0.125 to 0.125
- value_weight: bfloat16 [2048, 2048], P('sp', 'tp'), may hold values from -0.125 to 0.125
- input_gate_weight: bfloat16 [2048, 8], P(None, 'tp'), may hold values from -0.125 to 0.125
- forget_gate_weight: bfloat16 [2048, 8], P(None, 'tp'), may hold values from -0.125 to 0.125
- input_offset: float32 [1024, 8], P('sp', 'tp'), may hold values from -4 to 210
- forget_offset: float32 [1024, 8], P('sp', 'tp'), may hold values from 0 to 30
- memory_norm_gain: float32 [2048], P('tp'), may hold values from 0.1 to 1.9
- conv_out_weight: bfloat16 [1024, 2048], P('tp', 'sp'), may hold values from -0.3125 to 0.3125
- memory_out_weight: bfloat16 [2048, 2048], P('tp', 'sp'), may hold values from -0.125 to 0.125
Outputs:
- mixed: bfloat16 [1024, 2048], P('sp', 'tp')
All inputs are finite; a program needn't handle non-finite values.
Results may differ from a plain program's by a relative error of at most 0.03.
Values may be sent and summed in bfloat16 or wider, within the bound.
A program may use at most 128 MiB of HBM per device.

v0:
```python
import jax
import jax.numpy as jnp
from jax import lax
from jax.sharding import PartitionSpec as P

BLOCK = 64
EPS = 1e-06
LOWEST_LEVEL = -1e30


def shifted_2(value, axis, steps):
    count = lax.axis_size(axis)
    leading, last = (max(0, -steps), min(count, count - steps))
    return lax.ppermute(value, axis, [(source, source + steps) for source in range(leading, last)])


def carried_in(shard, axis, join, neutral):
    place = lax.axis_index(axis)
    gathered = jax.tree.map(
        lambda a, kind: lax.all_gather(a.astype(kind), axis),
        shard,
        (jnp.bfloat16, jnp.bfloat16, jnp.bfloat16, jnp.bfloat16),
    )
    state = jax.tree.map(lambda a, e: jnp.zeros_like(a) + jnp.asarray(e, a.dtype), shard, neutral)

    def one(step, state):
        return join(
            state,
            jax.tree.map(
                lambda a, own: lax.dynamic_index_in_dim(a, step, 0, False).astype(own.dtype),
                gathered,
                shard,
            ),
        )

    return lax.fori_loop(0, place, one, state)


def block_step(carry, inputs):
    state, normal, level = carry
    query, key, value, gate_in, forget_log = inputs
    length = gate_in.shape[-1]
    scale = query.shape[-1] ** (-0.5)
    causal = jnp.tril(jnp.ones((length, length), dtype=bool))
    within = jnp.cumsum(forget_log, axis=-1)
    log_weight = within[:, :, None] - within[:, None, :] + gate_in[:, None, :]
    log_weight = jnp.where(causal, log_weight, -jnp.inf)
    carried = within + level[:, None]
    top = jnp.maximum(carried, jnp.max(log_weight, axis=-1))
    weight = jnp.exp(log_weight - top[:, :, None])
    carried_weight = jnp.exp(carried - top) * scale
    scores = jnp.einsum("htd,hsd->hts", query, key, preferred_element_type=jnp.float32) * (
        scale * weight
    )
    numer = jnp.einsum(
        "hts,hse->hte", scores.astype(jnp.bfloat16), value, preferred_element_type=jnp.float32
    )
    numer = numer + carried_weight[:, :, None] * jnp.einsum(
        "hed,htd->hte", state.astype(jnp.bfloat16), query, preferred_element_type=jnp.float32
    )
    denom = jnp.sum(scores, axis=-1) + carried_weight * jnp.einsum(
        "hd,htd->ht", normal.astype(jnp.bfloat16), query, preferred_element_type=jnp.float32
    )
    result = numer / jnp.maximum(jnp.abs(denom), 1.0)[:, :, None]
    last = within[:, -1]
    end_log = last[:, None] - within + gate_in
    new_level = jnp.maximum(last + level, jnp.max(end_log, axis=-1))
    keep = jnp.exp(last + level - new_level)
    fresh = jnp.exp(end_log - new_level[:, None])
    scaled_key = (fresh[:, :, None] * key).astype(jnp.bfloat16)
    new_state = keep[:, None, None] * state + jnp.einsum(
        "hse,hsd->hed", value, scaled_key, preferred_element_type=jnp.float32
    )
    new_normal = keep[:, None] * normal + jnp.sum(scaled_key.astype(jnp.float32), axis=1)
    return ((new_state, new_normal, new_level), result)


def depthwise(extended, kernel):
    taps = kernel.shape[0]
    length = extended.shape[0] - taps + 1
    total = extended[0:length] * kernel[0]
    for index in range(1, taps):
        total = total + extended[index : index + length] * kernel[index]
    return total


def merge_states(first, second):
    first_state, first_normal, first_level, first_total = first
    second_state, second_normal, second_level, second_total = second
    shifted = first_level + second_total
    level = jnp.maximum(shifted, second_level)
    older = jnp.exp(shifted - level)
    newer = jnp.exp(second_level - level)
    state = older[:, None, None] * first_state + newer[:, None, None] * second_state
    normal = older[:, None] * first_normal + newer[:, None] * second_normal
    return (state, normal, level, first_total + second_total)


def on_device(
    tokens,
    conv_value_weight,
    conv_gate_weight,
    conv_kernel,
    conv_norm_gain,
    query_weight,
    key_weight,
    value_weight,
    input_gate_weight,
    forget_gate_weight,
    input_offset,
    forget_offset,
    memory_norm_gain,
    conv_out_weight,
    memory_out_weight,
):
    length = tokens.shape[0]
    heads_here = input_gate_weight.shape[1]
    whole = lax.all_gather(tokens, "tp", axis=1, tiled=True)
    pieces = (
        lax.all_gather(conv_value_weight, "sp", axis=0, tiled=True),
        lax.all_gather(conv_gate_weight, "sp", axis=0, tiled=True),
        lax.all_gather(query_weight, "sp", axis=0, tiled=True),
        lax.all_gather(key_weight, "sp", axis=0, tiled=True),
        lax.all_gather(value_weight, "sp", axis=0, tiled=True),
    )
    folded = tuple((jnp.dot(whole, piece, preferred_element_type=jnp.float32) for piece in pieces))
    conv_value, conv_gate, query_flat, key_flat, value_flat = folded
    gate_pre = jnp.dot(whole, input_gate_weight, preferred_element_type=jnp.float32)
    forget_pre = jnp.dot(whole, forget_gate_weight, preferred_element_type=jnp.float32)
    glu = (conv_value * jax.nn.sigmoid(conv_gate)).astype(jnp.bfloat16)
    taps = conv_kernel.shape[0]
    head_dim = query_flat.shape[1] // heads_here

    def to_heads(flat):
        return flat.astype(jnp.bfloat16).reshape(length, heads_here, head_dim).transpose(1, 0, 2)

    query = to_heads(query_flat)
    key = to_heads(key_flat)
    value = to_heads(value_flat)
    gate_in = (gate_pre + input_offset).T
    forget_log = jax.nn.log_sigmoid(forget_pre + forget_offset).T
    within = jnp.cumsum(forget_log, axis=1)
    total = within[:, -1]
    end_log = total[:, None] - within + gate_in
    local_level = jnp.max(end_log, axis=1)
    fresh = jnp.exp(end_log - local_level[:, None])
    scaled_key = (fresh[:, :, None] * key).astype(jnp.bfloat16)
    local_state = jnp.einsum("hse,hsd->hed", value, scaled_key, preferred_element_type=jnp.float32)
    local_normal = jnp.sum(scaled_key.astype(jnp.float32), axis=1)
    blank_state = (
        jnp.zeros_like(local_state),
        jnp.zeros_like(local_normal),
        jnp.full_like(local_level, LOWEST_LEVEL),
        jnp.zeros_like(total),
    )
    prior = shifted_2(glu[length - (taps - 1) :], "sp", 1)
    incoming = carried_in(
        (local_state, local_normal, local_level, total), "sp", merge_states, blank_state
    )
    extended = jnp.concatenate([prior, glu], axis=0).astype(jnp.float32)
    conv = depthwise(extended, conv_kernel.astype(jnp.float32))
    blocks = length // BLOCK

    def split(array):
        return jnp.moveaxis(array.reshape((heads_here, blocks, BLOCK) + array.shape[2:]), 1, 0)

    _, hidden = lax.scan(
        block_step,
        tuple(incoming[:3]),
        (split(query), split(key), split(value), split(gate_in), split(forget_log)),
    )
    hidden = jnp.moveaxis(hidden, 0, 1).reshape(heads_here, length, head_dim)
    hidden_squares = jnp.sum(hidden * hidden, axis=(0, 2))
    channel_sum, channel_squares, memory_squares = lax.psum(
        (jnp.sum(conv, axis=1), jnp.sum(conv * conv, axis=1), hidden_squares), "tp"
    )
    channels = conv.shape[1] * lax.axis_size("tp")
    mean = (channel_sum / channels)[:, None]
    variance = (channel_squares / channels)[:, None] - mean * mean
    conv_branch = jax.nn.silu((conv - mean) * lax.rsqrt(variance + EPS) * conv_norm_gain).astype(
        jnp.bfloat16
    )
    entries = heads_here * head_dim * lax.axis_size("tp")
    memory_scale = lax.rsqrt(memory_squares / entries + EPS)
    hidden = hidden * memory_scale[None, :, None]
    hidden = hidden * memory_norm_gain.reshape(heads_here, 1, head_dim)
    memory_branch = (
        hidden.transpose(1, 0, 2).reshape(length, heads_here * head_dim).astype(jnp.bfloat16)
    )
    conv_columns, memory_columns = (
        lax.all_gather(conv_out_weight, "sp", axis=1, tiled=True),
        lax.all_gather(memory_out_weight, "sp", axis=1, tiled=True),
    )
    contract = (((0,), (1,)), ((), ()))
    summed = lax.psum_scatter(
        (
            lax.dot_general(conv_columns, conv_branch, contract, preferred_element_type=jnp.float32)
            + lax.dot_general(
                memory_columns, memory_branch, contract, preferred_element_type=jnp.float32
            )
        ).astype(jnp.bfloat16),
        "tp",
        scatter_dimension=0,
        tiled=True,
    ).astype(jnp.float32)
    return summed.T.astype(jnp.bfloat16)


def solution(mesh):
    in_specs = (
        P("sp", "tp"),
        P("sp", "tp"),
        P("sp", "tp"),
        P(None, "tp"),
        P("tp"),
        P("sp", "tp"),
        P("sp", "tp"),
        P("sp", "tp"),
        P(None, "tp"),
        P(None, "tp"),
        P("sp", "tp"),
        P("sp", "tp"),
        P("tp"),
        P("tp", "sp"),
        P("tp", "sp"),
    )
    out_specs = P("sp", "tp")
    return jax.shard_map(
        on_device, mesh=mesh, in_specs=in_specs, out_specs=out_specs, check_vma=False
    )
```

profile of v0, /device:TPU:0, one launch (start us, length us, event | category | flops | bytes accessed | tf_op | source)
XLA Modules:
  0.0 414.2 jit_solution(13057960020475259592)
XLA Ops:
  6.5 0.7 all-gather.22.cloned.1.call-update
  7.3 0.7 all-gather.20.cloned.1.call-update
  8.1 0.7 all-gather.14.cloned.1.call-update
  8.8 0.5 all-gather.16.cloned.1.call-update
  9.4 0.5 all-gather.24.cloned.1.call-update
  10.0 8.9 %all_gather.44 = bf16[128,2048]{1,0:T(8,128)(2,1)S(1)} all-gather(bf16[128,512]{1,0:T(8,128)(2,1)} %param.19), channel_id=1, replica_groups=mesh['sp'=8,'tp'=4] {'tp'}, dimensions={1}, use_global_device_ids=true | all-gather | bytes 655360 | tf_op jit(solution)/shard_map/all_gather | solution.py:118
  18.8 1.0 fusion.87
  19.8 0.3 reduce_window_sum.22
  20.1 0.2 slice_reduce_fusion.1
  20.3 0.4 fusion.94
  20.8 41.0 %all-gather.22.cloned.1.call-done = bf16[2048,512]{1,0:T(8,128)(2,1)} async-done(((bf16[256,512]{1,0:T(8,128)(2,1)}), bf16[2048,512]{1,0:T(8,128)(2,1)}) %all-gather.22.cloned.1.call-update) | async-done | bytes 2097168 | tf_op jit(solution)/shard_map/all_gather | solution.py:123
  61.7 2.0 convolution_convert_fusion.2
  63.8 47.7 %all-gather.20.cloned.1.call-done = bf16[2048,512]{1,0:T(8,128)(2,1)} async-done(((bf16[256,512]{1,0:T(8,128)(2,1)}), bf16[2048,512]{1,0:T(8,128)(2,1)}) %all-gather.20.cloned.1.call-update) | async-done | bytes 2097168 | tf_op jit(solution)/shard_map/all_gather | solution.py:124
  111.5 2.0 convolution_convert_fusion.3
  113.5 1.0 convolution_convert_fusion
  114.7 0.7 all-gather.18.cloned.1.call-update
  115.4 0.7 all-gather.26.cloned.1.call-update
  116.2 0.2 fusion.88
  116.4 0.6 dynamic-slice
  117.7 0.2 dynamic-update-slice.1
  117.9 0.2 dynamic-update-slice
  118.1 34.3 %all-gather.14.cloned.1.call-done = bf16[2048,256]{1,0:T(8,128)(2,1)} async-done(((bf16[256,256]{1,0:T(8,128)(2,1)}), bf16[2048,256]{1,0:T(8,128)(2,1)}) %all-gather.14.cloned.1.call-update) | async-done | bytes 1048592 | tf_op jit(solution)/shard_map/all_gather | solution.py:120
  152.5 1.5 fusion.99
  154.0 39.5 %all-gather.16.cloned.1.call-done = bf16[2048,256]{1,0:T(8,128)(2,1)} async-done(((bf16[256,256]{1,0:T(8,128)(2,1)}), bf16[2048,256]{1,0:T(8,128)(2,1)}) %all-gather.16.cloned.1.call-update) | async-done | bytes 1048592 | tf_op jit(solution)/shard_map/all_gather | solution.py:121
  193.5 1.6 fusion.43
  195.1 2.5 collective-permute-start
  197.6 18.5 %all-reduce.3 = (bf16[16]{0:T(256)(128)(2,1)S(1)}, bf16[16]{0:T(256)(128)(2,1)S(1)}) all-reduce(bf16[16]{0:T(256)(128)(2,1)S(1)} %dynamic-update-slice, bf16[16]{0:T(256)(128)(2,1)S(1)} %dynamic-update-slice.1), channel_id=2, replica_groups=mesh['sp'=8,'tp'=4] {'sp'}, use_global_device_ids=true, to_apply=%add | all-reduce | flops 32 | bytes 128
  216.2 0.1 reshape.176
  216.5 0.6 fusion.90
  217.0 0.1 fusion.80
  217.2 17.5 %all-gather.4 = bf16[8,2,256]{2,1,0:T(2,128)(2,1)S(1)} all-gather(bf16[1,2,256]{2,1,0:T(2,128)(2,1)S(1)} %bitcast.242), channel_id=5, replica_groups=mesh['sp'=8,'tp'=4] {'sp'}, dimensions={0}, use_global_device_ids=true | all-gather | bytes 9216 | tf_op jit(solution)/shard_map/all_gather | solution.py:20
  234.7 8.8 %all-gather.24.cloned.1.call-done = bf16[2048,512]{1,0:T(8,128)(2,1)} async-done(((bf16[256,512]{1,0:T(8,128)(2,1)}), bf16[2048,512]{1,0:T(8,128)(2,1)}) %all-gather.24.cloned.1.call-update) | async-done | bytes 2097168 | tf_op jit(solution)/shard_map/all_gather | solution.py:122
  243.5 2.0 convolution_convert_fusion.1
  245.6 47.6 %all-gather.28.cloned.1.call-done = bf16[16,256,256]{2,1,0:T(8,128)(2,1)} async-done(((bf16[2,256,256]{2,1,0:T(8,128)(2,1)}), bf16[16,256,256]{2,1,0:T(8,128)(2,1)}) %all-gather.28.cloned.1.call-update) | async-done | bytes 2097168 | tf_op jit(solution)/shard_map/all_gather | solution.py:20
  293.3 4.7 %while.33 = (s32[]{:T(128)}, f32[2,256,256]{2,1,0:T(8,128)S(1)}, f32[2,256]{1,0:T(2,128)S(1)}, f32[2]{0:T(128)S(1)}, f32[2,2,64,256]{3,2,0,1:T(8,128)S(1)}, /*in...) while((s32[]{:T(128)}, f32[2,256,256]{2,1,0:T(8,128)S(1)}, ...), condition=%wide.region_15.16_spmd, body=%wide.region_9.15_spmd.sunk | while | flops 42875268 | bytes 2589957 | solution.py:167
  293.3 0.2 reduce_window_sum.24
  293.5 0.2 slice_reduce_fusion.3
  293.7 0.2 fusion.144
  293.9 0.1 fusion.145
  294.1 0.2 fusion.146
  294.3 0.2 fusion.147
  294.6 0.1 convert_reduce_fusion.2
  294.8 0.1 fusion.148
  295.0 0.2 fusion.149
  295.2 0.4 convolution_add_fusion.5
  295.6 0.2 reduce_window_sum.24
  295.9 0.2 slice_reduce_fusion.3
  296.1 0.2 fusion.144
  296.3 0.1 fusion.145
  296.5 0.2 fusion.146
  296.6 0.2 fusion.147
  296.9 0.1 convert_reduce_fusion.2
  297.1 0.1 fusion.148
  297.3 0.2 fusion.149
  297.6 0.4 convolution_add_fusion.5
  298.0 0.1 fusion.48
  298.2 5.6 %all-reduce.2 = (f32[128]{0:T(128)S(1)}, f32[128]{0:T(128)S(1)}, f32[128]{0:T(128)S(1)}) all-reduce(f32[128]{0:T(128)S(1)} %get-tuple-element.156, f32[128]{0:T(128)S(1)} %get-tuple-element.155, f32[128]{0:T(128)S(1)} %reduce_sum.63), channel_id=1, replica_groups=mesh['sp'=8,'tp'=4] {'tp'}, use_global_device_ids=true, to_apply=%region_3.4 | all-reduce | flops 384 | bytes 3072 | tf_op jit(solution)/shard_map/psum | solution.py:174
  303.8 0.1 fusion.47
  303.9 0.1 copy.44
  304.1 29.3 %all-gather.18.cloned.1.call-done = bf16[256,2048]{1,0:T(8,128)(2,1)} async-done(((bf16[256,256]{1,0:T(8,128)(2,1)}), bf16[256,2048]{1,0:T(8,128)(2,1)}) %all-gather.18.cloned.1.call-update) | async-done | bytes 1048592 | tf_op jit(solution)/shard_map/all_gather | solution.py:191
  333.4 1.6 fusion.81
  335.0 49.8 %all-gather.26.cloned.1.call-done = bf16[512,2048]{1,0:T(8,128)(2,1)} async-done(((bf16[512,256]{1,0:T(8,128)(2,1)}), bf16[512,2048]{1,0:T(8,128)(2,1)}) %all-gather.26.cloned.1.call-update) | async-done | bytes 2097168 | tf_op jit(solution)/shard_map/all_gather | solution.py:192
  384.8 2.9 fusion.38
  387.7 20.0 %reduce-scatter.2.cloned.1.call-done = bf16[512,128]{0,1:T(8,128)(2,1)} async-done(((bf16[2048,128]{0,1:T(8,128)(2,1)}), bf16[512,128]{0,1:T(8,128)(2,1)}) %reduce-scatter.2.cloned.1.call-update) | async-done | bytes 131088 | tf_op jit(solution)/shard_map/reduce_scatter | solution.py:195
  (65 shorter events, 1.6 us)
Async XLA Ops:
  6.5 13.8 %copy-start = (bf16[2048,2]{0,1:T(2,128)(2,1)S(1)}, bf16[2048,2]{0,1:T(2,128)(2,1)}, u32[]{:S(2)}) copy-start(bf16[2048,2]{0,1:T(2,128)(2,1)} %param.27) | copy-start | bytes 24580
  6.5 13.8 %copy-start.4 = (f32[128,2]{0,1:T(2,128)S(1)}, f32[128,2]{0,1:T(2,128)}, u32[]{:S(2)}) copy-start(f32[128,2]{0,1:T(2,128)} %param.29) | copy-start | bytes 3076
  6.5 55.2 %all-gather.22.cloned.1.call-start = ((), (), s32[]{:S(2)}) async-start(), calls=%async_computation.5 | async-start | bytes 2359296 | tf_op jit(solution)/shard_map/all_gather | solution.py:123
  7.3 104.2 %all-gather.20.cloned.1.call-start = ((), (), s32[]{:S(2)}) async-start(), calls=%async_computation.4 | async-start | bytes 2359296 | tf_op jit(solution)/shard_map/all_gather | solution.py:124
  8.0 144.5 %all-gather.14.cloned.1.call-start = ((), (), s32[]{:S(2)}) async-start(), calls=%async_computation.1 | async-start | bytes 1179648 | tf_op jit(solution)/shard_map/all_gather | solution.py:120
  8.7 184.7 %all-gather.16.cloned.1.call-start = ((), (), s32[]{:S(2)}) async-start(), calls=%async_computation.2 | async-start | bytes 1179648 | tf_op jit(solution)/shard_map/all_gather | solution.py:121
  9.3 234.2 %all-gather.24.cloned.1.call-start = ((), (), s32[]{:S(2)}) async-start(), calls=%async_computation.6 | async-start | bytes 2359296 | tf_op jit(solution)/shard_map/all_gather | solution.py:122
  9.9 283.3 %all-gather.28.cloned.1.call-start = ((), (), s32[]{:S(2)}) async-start(), calls=%async_computation.9 | async-start | bytes 2359296 | tf_op jit(solution)/shard_map/all_gather | solution.py:20
  63.8 52.6 %copy-start.1 = (bf16[31,256]{1,0:T(8,128)(2,1)S(1)}, bf16[31,256]{1,0:T(8,128)(2,1)}, u32[]{:S(2)}) copy-start(bf16[31,256]{1,0:T(8,128)(2,1)} %param.22) | copy-start | bytes 47620
  63.8 52.6 %copy-start.5 = (u32[32]{0:T(128)S(1)}, u32[32]{0:T(128)}, u32[]{:S(2)}) copy-start(u32[32]{0:T(128)} %constant.96) | copy-start | bytes 388
  114.6 101.8 %copy-start.2 = (f32[512]{0:T(512)S(1)}, f32[512]{0:T(512)}, u32[]{:S(2)}) copy-start(f32[512]{0:T(512)} %param.31) | copy-start | bytes 6148
  114.6 218.8 %all-gather.18.cloned.1.call-start = ((), (), s32[]{:S(2)}) async-start(), calls=%async_computation.3 | async-start | bytes 1179648 | tf_op jit(solution)/shard_map/all_gather | solution.py:191
  115.4 269.5 %all-gather.26.cloned.1.call-start = ((), (), s32[]{:S(2)}) async-start(), calls=%async_computation.7 | async-start | bytes 2359296 | tf_op jit(solution)/shard_map/all_gather | solution.py:192
  116.1 291.6 %reduce-scatter.2.cloned.1.call-start = ((), (), s32[]{:S(2)}) async-start(), calls=%async_computation.8 | async-start | bytes 655360 | tf_op jit(solution)/shard_map/reduce_scatter | solution.py:195
  195.1 21.4 %collective-permute-start = (bf16[30,256]{1,0:T(8,128)(2,1)S(1)}, bf16[30,256]{1,0:T(8,128)(2,1)S(1)}, u32[]{:S(2)}, u32[]{:S(2)}) collective-permute-start(bf16[30,256]{1,0:T(8,128)(2,1)S(1)} %slice.259), channel_id=1, source_target_pairs={{0,4},{4,8},{8,12},{12,16},{16,20},{20,24},{24,28},{1,5},{5,9},{9,... | collective-permute-start | bytes 46088 | tf_op jit(solution)/shard_map/ppermute | solution.py:14
  293.3 40.1 %copy-start.3 = (f32[256]{0:T(256)S(1)}, f32[256]{0:T(256)}, u32[]{:S(2)}) copy-start(f32[256]{0:T(256)} %param.23) | copy-start | bytes 3076
Sparse Core Ops, SparseCore 0:
  9.5 52.2 all-gather.21
  63.8 47.6 all-gather.19
  113.6 38.7 all-gather.13
  154.5 38.9 all-gather.15
  195.4 48.0 all-gather.23
  245.5 47.6 all-gather.27
  295.2 38.1 all-gather.17
  335.4 49.3 all-gather.25
  387.8 19.8 reduce-scatter.1
where the time goes:
time: 415 us; the launch traced here: 414 us
  waiting for transfers between devices  323 us (78%)
  blocking collectives  50.5 us (12%)
  matrix products  18.2 us (4%)
  between operations  14.1 us (3%)
    all_gather x1, waiting for transfers between devices, on_device(): lax.all_gather(memory_out_weight, 'sp', axis=1, tiled=True)  49.8 us
    all_gather x1, waiting for transfers between devices, on_device(): lax.all_gather(value_weight, 'sp', axis=0, tiled=True)  47.7 us
    all_gather x1, waiting for transfers between devices, carried_in(): lax.all_gather(a.astype(kind), axis)  47.6 us
    all_gather x1, waiting for transfers between devices, on_device(): lax.all_gather(key_weight, 'sp', axis=0, tiled=True)  41 us
    all_gather x1, waiting for transfers between devices, on_device(): lax.all_gather(conv_gate_weight, 'sp', axis=0, tiled=True)  39.5 us
    all_gather x1, waiting for transfers between devices, on_device(): lax.all_gather(conv_value_weight, 'sp', axis=0, tiled=True)  34.3 us
    all_gather x1, waiting for transfers between devices, on_device(): lax.all_gather(conv_out_weight, 'sp', axis=1, tiled=True)  29.3 us
    reduce_scatter x1, waiting for transfers between devices, on_device(): lax.psum_scatter((lax.dot_general(conv_columns, conv_branch, contract, pr...  20 us
  transfers between devices with their start and end apart: 10, of which 9 were waited for; matrix products, arithmetic and copies ran while one was open for 5% of the time, Pallas kernels for 0%

commit v1 on v0

--- a/solution.py
+++ b/solution.py
@@ -6,6 +6,11 @@
 BLOCK = 64
 EPS = 1e-06
 LOWEST_LEVEL = -1e30
+
+
+def all_parts(value, mesh_axis, dim):
+    tiles = lax.all_gather(value, mesh_axis)
+    return jnp.concatenate(tiles, axis=dim)
 
 
 def shifted_2(value, axis, steps):
@@ -189,7 +194,7 @@
     )
     conv_columns, memory_columns = (
         lax.all_gather(conv_out_weight, "sp", axis=1, tiled=True),
-        lax.all_gather(memory_out_weight, "sp", axis=1, tiled=True),
+        all_parts(memory_out_weight, "sp", 1),
     )
     contract = (((0,), (1,)), ((), ()))
     summed = lax.psum_scatter(

time: 415 us -> 414 us (level)
  no operation moved by 1% of the time
where the time goes in v1:
time: 414 us
  waiting for transfers between devices  320 us (77%)
  blocking collectives  50.5 us (12%)
  matrix products  17 us (4%)
  between operations  14.1 us (3%)
  local copies, waits for them, and re-layouts  5.38 us (1%)
    all_gather x1, waiting for transfers between devices, on_device(): lax.all_gather(value_weight, 'sp', axis=0, tiled=True)  47.7 us
    all_gather x1, waiting for transfers between devices, all_parts(): tiles = lax.all_gather(value, mesh_axis)  47.6 us
    all_gather x1, waiting for transfers between devices, carried_in(): lax.all_gather(a.astype(kind), axis)  46.9 us
    all_gather x1, waiting for transfers between devices, on_device(): lax.all_gather(key_weight, 'sp', axis=0, tiled=True)  40 us
    all_gather x1, waiting for transfers between devices, on_device(): lax.all_gather(conv_gate_weight, 'sp', axis=0, tiled=True)  39.5 us
    all_gather x1, waiting for transfers between devices, on_device(): lax.all_gather(conv_value_weight, 'sp', axis=0, tiled=True)  35.2 us
    all_gather x1, waiting for transfers between devices, on_device(): lax.all_gather(conv_out_weight, 'sp', axis=1, tiled=True)  29.3 us
    reduce_scatter x1, waiting for transfers between devices, on_device(): lax.psum_scatter((lax.dot_general(conv_columns, conv_branch, contract, pr...  20.9 us
  transfers between devices with their start and end apart: 10, of which 9 were waited for; matrix products, arithmetic and copies ran while one was open for 5% of the time, Pallas kernels for 0%

profile of v1, /device:TPU:0, one launch (start us, length us, event | category | flops | bytes accessed | tf_op | source)
XLA Modules:
  0.0 413.7 jit_solution(13394603774401688658)
XLA Ops:
  6.5 0.7 all-gather.23.cloned.1.call-update
  7.3 0.7 all-gather.21.cloned.1.call-update
  8.1 0.7 all-gather.15.cloned.1.call-update
  8.8 0.5 all-gather.17.cloned.1.call-update
  9.4 0.5 all-gather.25.cloned.1.call-update
  10.0 0.5 all-gather.29.cloned.1.call-update
  10.5 8.9 %all_gather.47 = bf16[128,2048]{1,0:T(8,128)(2,1)S(1)} all-gather(bf16[128,512]{1,0:T(8,128)(2,1)} %param.19), channel_id=1, replica_groups=mesh['sp'=8,'tp'=4] {'tp'}, dimensions={1}, use_global_device_ids=true | all-gather | bytes 655360 | tf_op jit(solution)/shard_map/all_gather | solution.py:123
  19.4 1.0 fusion.87
  20.4 0.3 reduce_window_sum.22
  20.7 0.2 slice_reduce_fusion.1
  20.9 0.4 fusion.94
  21.3 40.0 %all-gather.23.cloned.1.call-done = bf16[2048,512]{1,0:T(8,128)(2,1)} async-done(((bf16[256,512]{1,0:T(8,128)(2,1)}), bf16[2048,512]{1,0:T(8,128)(2,1)}) %all-gather.23.cloned.1.call-update) | async-done | bytes 2097168 | tf_op jit(solution)/shard_map/all_gather | solution.py:128
  61.4 2.0 convolution_convert_fusion.2
  63.4 47.7 %all-gather.21.cloned.1.call-done = bf16[2048,512]{1,0:T(8,128)(2,1)} async-done(((bf16[256,512]{1,0:T(8,128)(2,1)}), bf16[2048,512]{1,0:T(8,128)(2,1)}) %all-gather.21.cloned.1.call-update) | async-done | bytes 2097168 | tf_op jit(solution)/shard_map/all_gather | solution.py:129
  111.1 2.0 convolution_convert_fusion.3
  113.2 1.0 convolution_convert_fusion
  114.3 0.7 all-gather.19.cloned.1.call-update
  115.1 0.2 fusion.88
  115.3 0.6 dynamic-slice
  116.5 0.2 dynamic-update-slice.1
  116.8 0.2 dynamic-update-slice
  117.0 35.2 %all-gather.15.cloned.1.call-done = bf16[2048,256]{1,0:T(8,128)(2,1)} async-done(((bf16[256,256]{1,0:T(8,128)(2,1)}), bf16[2048,256]{1,0:T(8,128)(2,1)}) %all-gather.15.cloned.1.call-update) | async-done | bytes 1048592 | tf_op jit(solution)/shard_map/all_gather | solution.py:125
  152.2 1.5 fusion.99
  153.7 39.5 %all-gather.17.cloned.1.call-done = bf16[2048,256]{1,0:T(8,128)(2,1)} async-done(((bf16[256,256]{1,0:T(8,128)(2,1)}), bf16[2048,256]{1,0:T(8,128)(2,1)}) %all-gather.17.cloned.1.call-update) | async-done | bytes 1048592 | tf_op jit(solution)/shard_map/all_gather | solution.py:126
  193.2 1.6 fusion.43
  194.8 2.5 collective-permute-start
  197.3 18.5 %all-reduce.3 = (bf16[16]{0:T(256)(128)(2,1)S(1)}, bf16[16]{0:T(256)(128)(2,1)S(1)}) all-reduce(bf16[16]{0:T(256)(128)(2,1)S(1)} %dynamic-update-slice, bf16[16]{0:T(256)(128)(2,1)S(1)} %dynamic-update-slice.1), channel_id=2, replica_groups=mesh['sp'=8,'tp'=4] {'sp'}, use_global_device_ids=true, to_apply=%add | all-reduce | flops 32 | bytes 128
  216.2 0.6 fusion.90
  216.7 0.1 fusion.80
  216.9 17.5 %all-gather.5 = bf16[8,2,256]{2,1,0:T(2,128)(2,1)S(1)} all-gather(bf16[1,2,256]{2,1,0:T(2,128)(2,1)S(1)} %bitcast.248), channel_id=5, replica_groups=mesh['sp'=8,'tp'=4] {'sp'}, dimensions={0}, use_global_device_ids=true | all-gather | bytes 9216 | tf_op jit(solution)/shard_map/all_gather | solution.py:25
  234.4 9.0 %all-gather.25.cloned.1.call-done = bf16[2048,512]{1,0:T(8,128)(2,1)} async-done(((bf16[256,512]{1,0:T(8,128)(2,1)}), bf16[2048,512]{1,0:T(8,128)(2,1)}) %all-gather.25.cloned.1.call-update) | async-done | bytes 2097168 | tf_op jit(solution)/shard_map/all_gather | solution.py:127
  243.4 2.0 convolution_convert_fusion.1
  245.5 47.6 %all-gather.29.cloned.1.call-done = bf16[4096,256]{1,0:T(8,128)(2,1)} async-done(((bf16[512,256]{1,0:T(8,128)(2,1)}), bf16[4096,256]{1,0:T(8,128)(2,1)}) %all-gather.29.cloned.1.call-update) | async-done | bytes 2097168 | tf_op jit(solution)/shard_map/all_gather | solution.py:12
  293.0 2.9 copy.58
  295.9 46.9 %all-gather.27.cloned.1.call-done = bf16[16,256,256]{2,1,0:T(8,128)(2,1)} async-done(((bf16[2,256,256]{2,1,0:T(8,128)(2,1)}), bf16[16,256,256]{2,1,0:T(8,128)(2,1)}) %all-gather.27.cloned.1.call-update) | async-done | bytes 2097168 | tf_op jit(solution)/shard_map/all_gather | solution.py:25
  342.9 4.7 %while.33 = (s32[]{:T(128)}, f32[2,256,256]{2,1,0:T(8,128)S(1)}, f32[2,256]{1,0:T(2,128)S(1)}, f32[2]{0:T(128)S(1)}, f32[2,2,64,256]{3,2,0,1:T(8,128)S(1)}, /*in...) while((s32[]{:T(128)}, f32[2,256,256]{2,1,0:T(8,128)S(1)}, ...), condition=%wide.region_15.16_spmd, body=%wide.region_9.15_spmd.sunk | while | flops 42875268 | bytes 2589957 | solution.py:172
  342.9 0.2 reduce_window_sum.24
  343.2 0.2 slice_reduce_fusion.3
  343.4 0.2 fusion.144
  343.6 0.1 fusion.145
  343.8 0.2 fusion.146
  343.9 0.2 fusion.147
  344.2 0.1 convert_reduce_fusion.2
  344.4 0.1 fusion.148
  344.6 0.2 fusion.149
  344.9 0.4 convolution_add_fusion.5
  345.3 0.2 reduce_window_sum.24
  345.5 0.2 slice_reduce_fusion.3
  345.7 0.2 fusion.144
  345.9 0.1 fusion.145
  346.1 0.2 fusion.146
  346.3 0.2 fusion.147
  346.6 0.1 convert_reduce_fusion.2
  346.8 0.1 fusion.148
  347.0 0.2 fusion.149
  347.2 0.4 convolution_add_fusion.5
  347.6 0.1 fusion.48
  347.8 5.6 %all-reduce.2 = (f32[128]{0:T(128)S(1)}, f32[128]{0:T(128)S(1)}, f32[128]{0:T(128)S(1)}) all-reduce(f32[128]{0:T(128)S(1)} %get-tuple-element.166, f32[128]{0:T(128)S(1)} %get-tuple-element.165, f32[128]{0:T(128)S(1)} %reduce_sum.63), channel_id=1, replica_groups=mesh['sp'=8,'tp'=4] {'tp'}, use_global_device_ids=true, to_apply=%region_3.4 | all-reduce | flops 384 | bytes 3072 | tf_op jit(solution)/shard_map/psum | solution.py:179
  353.4 0.1 fusion.47
  353.6 0.1 copy.57
  353.7 29.3 %all-gather.19.cloned.1.call-done = bf16[256,2048]{1,0:T(8,128)(2,1)} async-done(((bf16[256,256]{1,0:T(8,128)(2,1)}), bf16[256,2048]{1,0:T(8,128)(2,1)}) %all-gather.19.cloned.1.call-update) | async-done | bytes 1048592 | tf_op jit(solution)/shard_map/all_gather | solution.py:196
  383.0 1.6 fusion.81
  384.6 1.6 fusion.38
  386.3 20.9 %reduce-scatter.2.cloned.1.call-done = bf16[512,128]{0,1:T(8,128)(2,1)} async-done(((bf16[2048,128]{0,1:T(8,128)(2,1)}), bf16[512,128]{0,1:T(8,128)(2,1)}) %reduce-scatter.2.cloned.1.call-update) | async-done | bytes 131088 | tf_op jit(solution)/shard_map/reduce_scatter | solution.py:200
  (66 shorter events, 1.7 us)
Async XLA Ops:
  6.5 14.3 %copy-start = (bf16[2048,2]{0,1:T(2,128)(2,1)S(1)}, bf16[2048,2]{0,1:T(2,128)(2,1)}, u32[]{:S(2)}) copy-start(bf16[2048,2]{0,1:T(2,128)(2,1)} %param.27) | copy-start | bytes 24580
  6.5 14.4 %copy-start.4 = (f32[128,2]{0,1:T(2,128)S(1)}, f32[128,2]{0,1:T(2,128)}, u32[]{:S(2)}) copy-start(f32[128,2]{0,1:T(2,128)} %param.29) | copy-start | bytes 3076
  6.5 54.8 %all-gather.23.cloned.1.call-start = ((), (), s32[]{:S(2)}) async-start(), calls=%async_computation.5 | async-start | bytes 2359296 | tf_op jit(solution)/shard_map/all_gather | solution.py:128
  7.3 103.9 %all-gather.21.cloned.1.call-start = ((), (), s32[]{:S(2)}) async-start(), calls=%async_computation.4 | async-start | bytes 2359296 | tf_op jit(solution)/shard_map/all_gather | solution.py:129
  8.0 144.2 %all-gather.15.cloned.1.call-start = ((), (), s32[]{:S(2)}) async-start(), calls=%async_computation.1 | async-start | bytes 1179648 | tf_op jit(solution)/shard_map/all_gather | solution.py:125
  8.7 184.4 %all-gather.17.cloned.1.call-start = ((), (), s32[]{:S(2)}) async-start(), calls=%async_computation.2 | async-start | bytes 1179648 | tf_op jit(solution)/shard_map/all_gather | solution.py:126
  9.3 234.1 %all-gather.25.cloned.1.call-start = ((), (), s32[]{:S(2)}) async-start(), calls=%async_computation.6 | async-start | bytes 2359296 | tf_op jit(solution)/shard_map/all_gather | solution.py:127
  9.9 283.1 %all-gather.29.cloned.1.call-start = ((), (), s32[]{:S(2)}) async-start(), calls=%async_computation.9 | async-start | bytes 2359296 | tf_op jit(solution)/shard_map/all_gather | solution.py:12
  10.5 332.3 %all-gather.27.cloned.1.call-start = ((), (), s32[]{:S(2)}) async-start(), calls=%async_computation.8 | async-start | bytes 2359296 | tf_op jit(solution)/shard_map/all_gather | solution.py:25
  63.4 51.8 %copy-start.1 = (bf16[31,256]{1,0:T(8,128)(2,1)S(1)}, bf16[31,256]{1,0:T(8,128)(2,1)}, u32[]{:S(2)}) copy-start(bf16[31,256]{1,0:T(8,128)(2,1)} %param.22) | copy-start | bytes 47620
  63.4 51.9 %copy-start.5 = (u32[32]{0:T(128)S(1)}, u32[32]{0:T(128)}, u32[]{:S(2)}) copy-start(u32[32]{0:T(128)} %constant.96) | copy-start | bytes 388
  114.2 101.9 %copy-start.2 = (f32[512]{0:T(512)S(1)}, f32[512]{0:T(512)}, u32[]{:S(2)}) copy-start(f32[512]{0:T(512)} %param.31) | copy-start | bytes 6148
  114.2 268.8 %all-gather.19.cloned.1.call-start = ((), (), s32[]{:S(2)}) async-start(), calls=%async_computation.3 | async-start | bytes 1179648 | tf_op jit(solution)/shard_map/all_gather | solution.py:196
  115.0 292.2 %reduce-scatter.2.cloned.1.call-start = ((), (), s32[]{:S(2)}) async-start(), calls=%async_computation.7 | async-start | bytes 655360 | tf_op jit(solution)/shard_map/reduce_scatter | solution.py:200
  194.8 21.4 %collective-permute-start = (bf16[30,256]{1,0:T(8,128)(2,1)S(1)}, bf16[30,256]{1,0:T(8,128)(2,1)S(1)}, u32[]{:S(2)}, u32[]{:S(2)}) collective-permute-start(bf16[30,256]{1,0:T(8,128)(2,1)S(1)} %slice.259), channel_id=1, source_target_pairs={{0,4},{4,8},{8,12},{12,16},{16,20},{20,24},{24,28},{1,5},{5,9},{9,... | collective-permute-start | bytes 46088 | tf_op jit(solution)/shard_map/ppermute | solution.py:19
  342.9 40.1 %copy-start.3 = (f32[256]{0:T(256)S(1)}, f32[256]{0:T(256)}, u32[]{:S(2)}) copy-start(f32[256]{0:T(256)} %param.23) | copy-start | bytes 3076
Sparse Core Ops, SparseCore 0:
  9.5 51.8 all-gather.22
  63.5 47.6 all-gather.20
  113.3 38.8 all-gather.14
  154.2 38.9 all-gather.16
  195.1 48.1 all-gather.24
  245.4 47.6 all-gather.28
  295.2 47.6 all-gather.26
  344.9 38.1 all-gather.18
  386.4 20.6 reduce-scatter.1
